TPU v7x, 128 devices: a whole 4x4x4 slice. The times are simulated.
128 devices in a mesh: sp: 16 (over z, y), tp: 8 (over x, core).
Axes of the slice: x: 4, y: 4, z: 4, core: 2. Of those that a mesh axis runs over, the one named last changes fastest.
Arguments:
- inputs: bfloat16 [16384, 2048], P(('sp', 'tp')), may hold values from -90 to 90
- in_gain: float32 [2048], replicated, may hold values from 0.1 to 1.9
- w_query: bfloat16 [2048, 1024], replicated, may hold values from -2 to 2
- w_key: bfloat16 [2048, 128], replicated, may hold values from -2 to 2
- w_value: bfloat16 [2048, 128], replicated, may hold values from -0.125 to 0.125
- query_gain: float32 [64], replicated, may hold values from 0 to 8, as said below
- key_gain: float32 [64], replicated, may hold values from 0 to 8, as said below
- decay_sums: float32 [16384, 16], P('sp', 'tp'), may hold values from -2343 to 0, as said below
- w_out: bfloat16 [1024, 2048], replicated, may hold values from -0.1875 to 0.1875
Outputs:
- result: bfloat16 [16384, 2048], P(('sp', 'tp'))
Inputs may be any that keep to these rules, and one draw needn't show every extreme that they name: `decay_sums`: along positions, each head's entries never rise. `query_gain`: every entry is positive. `key_gain`: every entry is positive.
All inputs are finite; a program needn't handle non-finite values.
Results may differ from a plain program's by a relative error of at most 0.015.
The roundings to bfloat16 on the way count: a program that leaves them out, or rounds other values in their place, can miss the bound.
Values may be sent and summed in bfloat16 or wider, within the bound.
A program may use at most 64 MiB of HBM per device.

v0:
```python
from functools import partial
import math
import jax
import jax.numpy as jnp
from jax import lax
from jax.sharding import Mesh
from jax.sharding import PartitionSpec as P

TP = ("tp_0", "tp_1")
SP_TP = ("sp", "tp_0", "tp_1")
epsilon = 1e-06


def joined_along(tiles, dim):
    tiles = jnp.moveaxis(tiles, 0, dim)
    lengths = tiles.shape
    return tiles.reshape(*lengths[:dim], lengths[dim] * lengths[dim + 1], *lengths[dim + 2 :])


def from_everyone(value, axis):
    length = lax.axis_size(axis)
    return lax.all_to_all(
        jnp.broadcast_to(value[None], (length, *value.shape)), axis, 0, 0, tiled=True
    )


def gathered_copies(value, axis, dim):
    return joined_along(from_everyone(value, axis), dim)


def partner(value, axis, stride):
    return lax.ppermute(value, axis, [(i, i ^ 1 << stride) for i in range(lax.axis_size(axis))])


def cut_along(value, dim, length):
    before, after = (value.shape[:dim], value.shape[dim + 1 :])
    return jnp.moveaxis(value.reshape(*before, length, -1, *after), dim, 0)


def moved_by_axis(tiles, axes, sequence):
    inside = tiles.shape[1:]
    filled = tiles.reshape(*(lax.axis_size(a) for a in axes), *inside)
    for k in sequence:
        filled = lax.all_to_all(filled, axes[k], k, k, tiled=True)
    return filled.reshape(-1, *inside)


def stepwise_exchange(value, axes, sequence, split_dim, concat_dim):
    tiles = cut_along(value, split_dim, lax.axis_size(axes))
    return joined_along(moved_by_axis(tiles, axes, sequence), concat_dim)


def rms_norm(vector, gain_vec):
    return (
        vector * lax.rsqrt(jnp.mean(vector * vector, axis=-1, keepdims=True) + epsilon) * gain_vec
    )


def attend_step(
    masked, query_rows, query_decay, query_pos, key_slice, value_slice, decay_slice, key_pos, inner
):
    peak, total, weighted = inner
    score_scale = query_rows.shape[2] ** (-0.5)
    scores = (
        jnp.einsum("thd,ud->htu", query_rows, key_slice, preferred_element_type=jnp.float32)
        * score_scale
    )
    scores = scores + query_decay[:, :, None] - decay_slice[:, None, :]
    if masked:
        visible = key_pos[None, :] <= query_pos[:, None]
        scores = jnp.where(visible[None], scores, -1e30)
    peak_new = jnp.maximum(peak, jnp.max(scores, axis=-1))
    weights_exp = jnp.exp(scores - peak_new[:, :, None])
    if masked:
        weights_exp = jnp.where(visible[None], weights_exp, 0.0)
    rescale = jnp.exp(peak - peak_new)
    total_new = total * rescale + jnp.sum(weights_exp, axis=-1)
    product = jnp.einsum(
        "htu,ud->thd",
        weights_exp.astype(jnp.bfloat16),
        value_slice,
        preferred_element_type=jnp.float32,
    )
    weighted_new = weighted * rescale.T[:, :, None] + product
    return (peak_new, total_new, weighted_new)


def keep_state(inner):
    return inner


def per_device(inputs, in_gain, w_query, w_key, w_value, query_gain, key_gain, decay_sums, w_out):
    tp_count = lax.axis_size(TP)
    sp_count = lax.axis_size("sp")
    sp_rank = lax.axis_index("sp")
    heads_dev = decay_sums.shape[1]
    head_size = query_gain.shape[0]
    kv_heads = w_key.shape[1] // head_size
    width_dev = heads_dev * head_size
    normed = rms_norm(inputs.astype(jnp.float32), in_gain).astype(jnp.bfloat16)
    row_count = normed.shape[0]
    all_heads = w_query.shape[1] // head_size
    query_all = rms_norm(
        jnp.dot(normed, w_query, preferred_element_type=jnp.float32).reshape(
            row_count, all_heads, head_size
        ),
        query_gain,
    ).astype(jnp.bfloat16)
    key_all = rms_norm(
        jnp.dot(normed, w_key, preferred_element_type=jnp.float32).reshape(
            row_count, kv_heads, head_size
        ),
        key_gain,
    ).astype(jnp.bfloat16)
    value_all = (
        jnp.dot(normed, w_value, preferred_element_type=jnp.float32)
        .astype(jnp.bfloat16)
        .reshape(row_count, kv_heads, head_size)
    )
    pair_all = jnp.repeat(
        jnp.concatenate([key_all, value_all], axis=2), tp_count // kv_heads, axis=1
    )
    packed = jnp.concatenate([query_all.reshape(row_count, tp_count, width_dev), pair_all], axis=2)
    received = lax.all_to_all(packed, TP, split_axis=1, concat_axis=0, tiled=True)[:, 0]
    tok_rows = received.shape[0]
    queries = received[:, :width_dev].reshape(tok_rows, heads_dev, head_size)
    key_values = received[:, width_dev:]
    all_decays = gathered_copies(decay_sums, "sp", 0)
    half_rows = tok_rows // 2
    bit_steps = sp_count.bit_length() - 1
    far_queries = queries[half_rows:]
    for bit in range(bit_steps):
        far_queries = partner(far_queries, "sp", bit)
    mirror = sp_count - 1 - sp_rank
    groups = [
        (queries[:half_rows], sp_rank * tok_rows),
        (far_queries, mirror * tok_rows + half_rows),
    ]
    prepared = []
    for query_rows, first_pos in groups:
        rows = query_rows.shape[0]
        query_decay = lax.dynamic_slice_in_dim(all_decays, first_pos, rows, 0).T
        query_pos = first_pos + jnp.arange(rows, dtype=jnp.int32)
        prepared.append((query_rows, query_decay, query_pos, first_pos, first_pos + rows - 1))
    initial = tuple(
        (
            (
                jnp.full((heads_dev, entry[0].shape[0]), -1e30, jnp.float32),
                jnp.zeros((heads_dev, entry[0].shape[0]), jnp.float32),
                jnp.zeros((entry[0].shape[0], heads_dev, head_size), jnp.float32),
            )
            for entry in prepared
        )
    )
    state = initial
    pieces = lax.all_gather(key_values, "sp", axis=0, tiled=True)
    piece_rows = pieces.shape[0]
    key_block = math.gcd(piece_rows, 512)

    def one_block(carry, block_index):
        key_start = block_index * key_block
        pair_slice = lax.dynamic_slice_in_dim(pieces, block_index * key_block, key_block, 0)
        key_slice = pair_slice[:, :head_size]
        value_slice = pair_slice[:, head_size:]
        decay_slice = lax.dynamic_slice_in_dim(all_decays, key_start, key_block, 0).T
        key_pos = key_start + jnp.arange(key_block, dtype=jnp.int32)
        updated = []
        for (query_rows, query_decay, query_pos, first_pos, last_pos), inner in zip(
            prepared, carry
        ):
            branch = jnp.where(
                key_start > last_pos, 0, jnp.where(key_start + key_block - 1 <= first_pos, 1, 2)
            )
            full_step = partial(
                attend_step,
                False,
                query_rows,
                query_decay,
                query_pos,
                key_slice,
                value_slice,
                decay_slice,
                key_pos,
            )
            masked_step = partial(
                attend_step,
                True,
                query_rows,
                query_decay,
                query_pos,
                key_slice,
                value_slice,
                decay_slice,
                key_pos,
            )
            updated.append(lax.switch(branch, [keep_state, full_step, masked_step], inner))
        return (tuple(updated), None)

    state, unused = lax.scan(one_block, state, jnp.arange(piece_rows // key_block, dtype=jnp.int32))
    outputs = [
        (weighted / total.T[:, :, None]).astype(jnp.bfloat16) for peak, total, weighted in state
    ]
    returned = outputs[1]
    for bit in range(bit_steps):
        returned = partner(returned, "sp", bit)
    attended = jnp.concatenate([outputs[0], returned], axis=0).reshape(tok_rows, width_dev)
    out_rows = stepwise_exchange(attended, TP, (1, 0), 0, 1)
    result = jnp.dot(out_rows, w_out, preferred_element_type=jnp.float32).astype(jnp.bfloat16)
    return result


def solution(mesh):
    torus = Mesh(mesh.devices.reshape(mesh.shape["sp"], 4, 2), ("sp", "tp_0", "tp_1"))
    in_specs = (P(SP_TP, None), P(), P(), P(), P(), P(), P(), P("sp", TP), P())
    out_specs = P(SP_TP, None)
    return jax.shard_map(
        per_device, mesh=torus, in_specs=in_specs, out_specs=out_specs, check_vma=False
    )
```

profile of v0, /device:TPU:24, one launch (start us, length us, event | category | flops | bytes accessed | tf_op | source)
XLA Modules:
  0.0 267.5 jit_solution(12323590933669240431)
XLA Ops:
  7.9 1.5 multiply_reduce_fusion
  9.4 1.6 convolution_convert_fusion.1
  11.0 3.0 %fusion.64 = (f32[128,1024]{1,0:T(8,128)S(1)}, f32[128,1024]{1,0:T(8,128)S(1)}) fusion(bf16[2048,1024]{1,0:T(8,128)(2,1)} %param.19, bf16[128,2048]{1,0:T(8,128)(2,1)S(1)} %copy-done.1, f32[2048]{0:T(1024)S(1)} %copy-done.2, f32[128]{0:T(128)S(1)} %add_rsqrt_fusion.2), kind=kOutput, calls=%fused_computation.100 | convolution fusion | flops 538050560 | bytes 5775872 | tf_op jit(solution)/shard_map/dot_general | solution.py:104
  15.1 14.5 %all_to_all.30 = bf16[128,8,256]{0,2,1:T(8,128)(2,1)S(1)} all-to-all(bf16[128,8,256]{0,2,1:T(8,128)(2,1)S(1)} %pad_maximum_fusion), channel_id=1, replica_groups=mesh['sp'=16,'tp_0'=4,'tp_1'=2] {'tp_0','tp_1'}, dimensions={1} | all-to-all | bytes 1048576 | tf_op jit(solution)/shard_map/all_to_all | solution.py:124
  31.5 4.3 %collective-permute-done = bf16[512,2,64]{0,2,1:T(8,128)(2,1)S(1)} collective-permute-done((bf16[512,2,64]{0,2,1:T(8,128)(2,1)S(1)}, bf16[512,2,64]{0,2,1:T(8,128)(2,1)S(1)}, u32[]{:S(2)}, u32[]{:S(2)}) %collective-permute-start) | collective-permute-done | bytes 131104 | tf_op jit(solution)/shard_map/ppermute | solution.py:32
  36.9 5.3 %collective-permute-done.1 = bf16[512,2,64]{0,2,1:T(8,128)(2,1)S(1)} collective-permute-done((bf16[512,2,64]{0,2,1:T(8,128)(2,1)S(1)}, bf16[512,2,64]{0,2,1:T(8,128)(2,1)S(1)}, u32[]{:S(2)}, u32[]{:S(2)}) %collective-permute-start.1) | collective-permute-done | bytes 131104 | tf_op jit(solution)/shard_map/ppermute | solution.py:32
  42.2 1.9 collective-permute-start.2
  44.8 8.9 %all-to-all-start.1 = ((f32[16,1024,2]{1,2,0:T(2,128)}), f32[16,1024,2]{1,2,0:T(2,128)S(1)}, u32[]{:S(2)}, u32[]{:S(2)}) async-start(f32[16,1024,2]{1,2,0:T(2,128)} %broadcast_in_dim.53), calls=%async_computation.1 | async-start | bytes 262144 | tf_op jit(solution)/shard_map/all_to_all | solution.py:22
  53.7 3.1 %collective-permute-start.3 = (bf16[512,2,64]{0,2,1:T(8,128)(2,1)S(1)}, bf16[512,2,64]{0,2,1:T(8,128)(2,1)S(1)}, u32[]{:S(2)}, u32[]{:S(2)}) collective-permute-start(bf16[512,2,64]{0,2,1:T(8,128)(2,1)S(1)} %collective-permute-done.2), channel_id=1, source_target_pairs={{0,64},{8,72},{16,80},{24,88},{32,96},{40,104},{48,112},{56,120},{... | collective-permute-start | bytes 393224 | tf_op jit(solution)/shard_map/ppermute | solution.py:32
  56.7 2.7 %all-to-all-done.1 = f32[16,1024,2]{1,2,0:T(2,128)S(1)} async-done(((f32[16,1024,2]{1,2,0:T(2,128)}), f32[16,1024,2]{1,2,0:T(2,128)S(1)}, u32[]{:S(2)}, u32[]{:S(2)}) %all-to-all-start.1) | async-done | bytes 131104 | tf_op jit(solution)/shard_map/all_to_all | solution.py:22
  60.6 23.3 %all-gather.2.cloned.1.call-done = bf16[16384,128]{1,0:T(8,128)(2,1)} async-done(((bf16[1024,128]{1,0:T(8,128)(2,1)}), bf16[16384,128]{1,0:T(8,128)(2,1)}) %all-gather.2.cloned.1.call-update) | async-done | bytes 4194320 | tf_op jit(solution)/shard_map/all_gather | solution.py:156
  84.0 133.3 %while.26 = (s32[]{:T(128)}, f32[2,512]{1,0:T(2,128)S(1)}, f32[2,512]{1,0:T(2,128)S(1)}, f32[512,2,64]{0,2,1:T(8,128)S(1)}, f32[2,512]{1,0:T(2,128)S(1)}, /*inde...) while((s32[]{:T(128)}, f32[2,512]{1,0:T(2,128)S(1)}, ...), condition=%wide.region_18.19_spmd.clone.clone, body=%wide.region_3.18_spmd.clone.clone.sunk | while | flops 280763904 | bytes 16956256 | solution.py:199
  86.6 1.4 conditional.9
  88.1 1.4 conditional.8
  92.1 1.4 conditional.9
  93.5 1.4 conditional.8
  99.0 1.4 conditional.8
  104.4 1.4 conditional.8
  109.9 1.4 conditional.8
  115.4 1.4 conditional.8
  120.8 2.1 conditional.8
  125.6 1.4 conditional.9
  129.7 1.4 conditional.9
  133.7 1.4 conditional.9
  137.8 1.4 conditional.9
  141.9 1.4 conditional.9
  146.0 1.4 conditional.9
  150.0 1.4 conditional.9
  154.1 1.4 conditional.9
  158.2 1.4 conditional.9
  162.3 1.4 conditional.9
  166.3 1.4 conditional.9
  170.4 1.4 conditional.9
  174.5 1.4 conditional.9
  178.6 1.4 conditional.9
  182.7 1.4 conditional.9
  186.7 1.4 conditional.9
  190.8 1.4 conditional.9
  194.9 1.4 conditional.9
  199.0 2.1 conditional.9
  218.3 4.2 %collective-permute-done.4 = bf16[512,2,64]{0,2,1:T(8,128)(2,1)S(1)} collective-permute-done((bf16[512,2,64]{0,2,1:T(8,128)(2,1)S(1)}, bf16[512,2,64]{0,2,1:T(8,128)(2,1)S(1)}, u32[]{:S(2)}, u32[]{:S(2)}) %collective-permute-start.4) | collective-permute-done | bytes 131104 | tf_op jit(solution)/shard_map/ppermute | solution.py:32
  222.5 1.4 collective-permute-start.5
  223.9 5.1 %collective-permute-done.5 = bf16[512,2,64]{0,2,1:T(8,128)(2,1)S(1)} collective-permute-done((bf16[512,2,64]{0,2,1:T(8,128)(2,1)S(1)}, bf16[512,2,64]{0,2,1:T(8,128)(2,1)S(1)}, u32[]{:S(2)}, u32[]{:S(2)}) %collective-permute-start.5) | collective-permute-done | bytes 131104 | tf_op jit(solution)/shard_map/ppermute | solution.py:32
  229.2 6.0 %collective-permute-done.6 = bf16[512,2,64]{0,2,1:T(8,128)(2,1)S(1)} collective-permute-done((bf16[512,2,64]{0,2,1:T(8,128)(2,1)S(1)}, bf16[512,2,64]{0,2,1:T(8,128)(2,1)S(1)}, u32[]{:S(2)}, u32[]{:S(2)}) %collective-permute-start.6) | collective-permute-done | bytes 131104 | tf_op jit(solution)/shard_map/ppermute | solution.py:32
  235.5 6.2 %collective-permute-done.7 = bf16[512,2,64]{0,2,1:T(8,128)(2,1)S(1)} collective-permute-done((bf16[512,2,64]{0,2,1:T(8,128)(2,1)S(1)}, bf16[512,2,64]{0,2,1:T(8,128)(2,1)S(1)}, u32[]{:S(2)}, u32[]{:S(2)}) %collective-permute-start.7) | collective-permute-done | bytes 131104 | tf_op jit(solution)/shard_map/ppermute | solution.py:32
  241.9 3.9 %all_to_all.31 = bf16[4,2,128,128]{2,3,0,1:T(8,128)(2,1)S(1)} all-to-all(bf16[4,2,128,128]{2,3,0,1:T(8,128)(2,1)S(1)} %copy.78), channel_id=1, replica_groups=mesh['sp'=16,'tp_0'=4,'tp_1'=2] {'tp_1'}, dimensions={1} | all-to-all | bytes 524288 | tf_op jit(solution)/shard_map/all_to_all | solution.py:44
  245.9 11.1 %all_to_all.32 = bf16[4,2,128,128]{2,3,1,0:T(8,128)(2,1)S(1)} all-to-all(bf16[4,2,128,128]{2,3,1,0:T(8,128)(2,1)S(1)} %copy.79), channel_id=1, replica_groups=mesh['sp'=16,'tp_0'=4,'tp_1'=2] {'tp_0'}, dimensions={0} | all-to-all | bytes 524288 | tf_op jit(solution)/shard_map/all_to_all | solution.py:44
  256.9 3.7 %convolution_convert_fusion = bf16[128,2048]{1,0:T(8,128)(2,1)} fusion(bf16[128,1024]{0,1:T(8,128)(2,1)S(1)} %bitcast.133, bf16[1024,2048]{1,0:T(8,128)(2,1)} %param.25), kind=kOutput, calls=%fused_computation.69 | convolution fusion | flops 537133056 | bytes 4980736 | tf_op jit(solution)/shard_map/dot_general | solution.py:208
  (550 shorter events, 122.5 us)
Async XLA Ops:
  6.5 1.3 copy-start
  6.5 4.4 %copy-start.1 = (bf16[128,2048]{1,0:T(8,128)(2,1)S(1)}, bf16[128,2048]{1,0:T(8,128)(2,1)}, u32[]{:S(2)}) copy-start(bf16[128,2048]{1,0:T(8,128)(2,1)} %param.17) | copy-start | bytes 1572868
  6.5 4.5 %copy-start.2 = (f32[2048]{0:T(1024)S(1)}, f32[2048]{0:T(1024)}, u32[]{:S(2)}) copy-start(f32[2048]{0:T(1024)} %param.18) | copy-start | bytes 24580
  6.5 77.4 %all-gather.2.cloned.1.call-start = ((), (), s32[]{:S(2)}) async-start(), calls=%async_computation.4 | async-start | bytes 4456448 | tf_op jit(solution)/shard_map/all_gather | solution.py:156
  14.0 0.7 copy-start.5
  14.0 0.7 copy-start.4
  15.1 29.1 %copy-start.3 = (f32[1024,2]{0,1:T(2,128)S(1)}, f32[1024,2]{0,1:T(2,128)}, u32[]{:S(2)}) copy-start(f32[1024,2]{0,1:T(2,128)} %param.24) | copy-start | bytes 24580
  30.6 5.1 %collective-permute-start = (bf16[512,2,64]{0,2,1:T(8,128)(2,1)S(1)}, bf16[512,2,64]{0,2,1:T(8,128)(2,1)S(1)}, u32[]{:S(2)}, u32[]{:S(2)}) collective-permute-start(bf16[512,2,64]{0,2,1:T(8,128)(2,1)S(1)} %bitcast.139), channel_id=1, source_target_pairs={{0,8},{8,0},{16,24},{24,16},{32,40},{40,32},{48,56},{56,48},{64,72... | collective-permute-start | bytes 393224 | tf_op jit(solution)/shard_map/ppermute | solution.py:32
  35.7 6.5 %collective-permute-start.1 = (bf16[512,2,64]{0,2,1:T(8,128)(2,1)S(1)}, bf16[512,2,64]{0,2,1:T(8,128)(2,1)S(1)}, u32[]{:S(2)}, u32[]{:S(2)}) collective-permute-start(bf16[512,2,64]{0,2,1:T(8,128)(2,1)S(1)} %collective-permute-done), channel_id=1, source_target_pairs={{0,16},{8,24},{16,0},{24,8},{32,48},{40,56},{48,32},{56,40},{64,80... | collective-permute-start | bytes 393224 | tf_op jit(solution)/shard_map/ppermute | solution.py:32
  42.2 11.5 %collective-permute-start.2 = (bf16[512,2,64]{0,2,1:T(8,128)(2,1)S(1)}, bf16[512,2,64]{0,2,1:T(8,128)(2,1)S(1)}, u32[]{:S(2)}, u32[]{:S(2)}) collective-permute-start(bf16[512,2,64]{0,2,1:T(8,128)(2,1)S(1)} %collective-permute-done.1), channel_id=1, source_target_pairs={{0,32},{8,40},{16,48},{24,56},{32,0},{40,8},{48,16},{56,24},{64,96... | collective-permute-start | bytes 393224 | tf_op jit(solution)/shard_map/ppermute | solution.py:32
  44.8 14.6 %all-to-all-start.1 = ((f32[16,1024,2]{1,2,0:T(2,128)}), f32[16,1024,2]{1,2,0:T(2,128)S(1)}, u32[]{:S(2)}, u32[]{:S(2)}) async-start(f32[16,1024,2]{1,2,0:T(2,128)} %broadcast_in_dim.53), calls=%async_computation.1 | async-start | bytes 262144 | tf_op jit(solution)/shard_map/all_to_all | solution.py:22
  53.7 6.9 %collective-permute-start.3 = (bf16[512,2,64]{0,2,1:T(8,128)(2,1)S(1)}, bf16[512,2,64]{0,2,1:T(8,128)(2,1)S(1)}, u32[]{:S(2)}, u32[]{:S(2)}) collective-permute-start(bf16[512,2,64]{0,2,1:T(8,128)(2,1)S(1)} %collective-permute-done.2), channel_id=1, source_target_pairs={{0,64},{8,72},{16,80},{24,88},{32,96},{40,104},{48,112},{56,120},{... | collective-permute-start | bytes 393224 | tf_op jit(solution)/shard_map/ppermute | solution.py:32
  217.4 5.1 %collective-permute-start.4 = (bf16[512,2,64]{0,2,1:T(8,128)(2,1)S(1)}, bf16[512,2,64]{0,2,1:T(8,128)(2,1)S(1)}, u32[]{:S(2)}, u32[]{:S(2)}) collective-permute-start(bf16[512,2,64]{0,2,1:T(8,128)(2,1)S(1)} %divide_convert_fusion), channel_id=1, source_target_pairs={{0,8},{8,0},{16,24},{24,16},{32,40},{40,32},{48,56},{56,48},{64,72... | collective-permute-start | bytes 393224 | tf_op jit(solution)/shard_map/ppermute | solution.py:32
  222.5 6.5 %collective-permute-start.5 = (bf16[512,2,64]{0,2,1:T(8,128)(2,1)S(1)}, bf16[512,2,64]{0,2,1:T(8,128)(2,1)S(1)}, u32[]{:S(2)}, u32[]{:S(2)}) collective-permute-start(bf16[512,2,64]{0,2,1:T(8,128)(2,1)S(1)} %collective-permute-done.4), channel_id=1, source_target_pairs={{0,16},{8,24},{16,0},{24,8},{32,48},{40,56},{48,32},{56,40},{64,80... | collective-permute-start | bytes 393224 | tf_op jit(solution)/shard_map/ppermute | solution.py:32
  229.0 6.2 %collective-permute-start.6 = (bf16[512,2,64]{0,2,1:T(8,128)(2,1)S(1)}, bf16[512,2,64]{0,2,1:T(8,128)(2,1)S(1)}, u32[]{:S(2)}, u32[]{:S(2)}) collective-permute-start(bf16[512,2,64]{0,2,1:T(8,128)(2,1)S(1)} %collective-permute-done.5), channel_id=1, source_target_pairs={{0,32},{8,40},{16,48},{24,56},{32,0},{40,8},{48,16},{56,24},{64,96... | collective-permute-start | bytes 393224 | tf_op jit(solution)/shard_map/ppermute | solution.py:32
  235.2 6.5 %collective-permute-start.7 = (bf16[512,2,64]{0,2,1:T(8,128)(2,1)S(1)}, bf16[512,2,64]{0,2,1:T(8,128)(2,1)S(1)}, u32[]{:S(2)}, u32[]{:S(2)}) collective-permute-start(bf16[512,2,64]{0,2,1:T(8,128)(2,1)S(1)} %collective-permute-done.6), channel_id=1, source_target_pairs={{0,64},{8,72},{16,80},{24,88},{32,96},{40,104},{48,112},{56,120},{... | collective-permute-start | bytes 393224 | tf_op jit(solution)/shard_map/ppermute | solution.py:32
Sparse Core Ops, SparseCore 0:
  30.6 53.2 all-gather.1
where the time goes:
time: 269 us; the launch traced here: 268 us
  local copies, waits for them, and re-layouts  63.6 us (24%)
  waiting for transfers between devices  58.1 us (22%)
  matrix products  43.4 us (16%)
  blocking collectives  29.4 us (11%)
  loops' own time  27.2 us (10%)
  starting transfers between devices  18.6 us (7%)
  between operations  13.7 us (5%)
  other arithmetic  13.4 us (5%)
    slice x32, local copies, waits for them, and re-layouts, one_block(): value_slice = pair_slice[:, head_size:]  35.1 us
    ppermute x8, waiting for transfers between devices, partner(): lax.ppermute(value, axis, [(i, i ^ 1 << stride) for i in range(lax.axis_s...  32 us
    another operation x1, loops' own time, per_device(): lax.scan(one_block, state, jnp.arange(piece_rows // key_block, dtype=jnp....  24.6 us
    all_gather x1, waiting for transfers between devices, per_device(): pieces = lax.all_gather(key_values, 'sp', axis=0, tiled=True)  23.3 us
    dynamic_slice x32, local copies, waits for them, and re-layouts, per_device(): lax.scan(one_block, state, jnp.arange(piece_rows // key_block, dtype=jnp....  18.8 us
    dot_general x33, matrix products, attend_step(): jnp.einsum('htu,ud->thd', weights_exp.astype(jnp.bfloat16), value_slice,...  17.1 us
    dot_general x33, matrix products, attend_step(): jnp.einsum('thd,ud->htu', query_rows, key_slice, preferred_element_type=j...  16.6 us
    all_to_all x2, blocking collectives, moved_by_axis(): filled = lax.all_to_all(filled, axes[k], k, k, tiled=True)  15 us
  transfers between devices with their start and end apart: 10, of which 9 were waited for; matrix products, arithmetic and copies ran while one was open for 0% of the time, Pallas kernels for 0%

commit v1 on v0

--- a/solution.py
+++ b/solution.py
@@ -153,7 +153,9 @@
         )
     )
     state = initial
-    pieces = lax.all_gather(key_values, "sp", axis=0, tiled=True)
+    pieces = jnp.concatenate(
+        lax.all_to_all(jnp.stack([key_values] * lax.axis_size("sp")), "sp", 0, 0), axis=0
+    )
     piece_rows = pieces.shape[0]
     key_block = math.gcd(piece_rows, 512)
 

time: 269 us -> 304 us (1.13)
  waiting for transfers between devices: 58.1 us -> 98.2 us
  between operations: 13.7 us -> 0.3 us
  local copies, waits for them, and re-layouts: 63.6 us -> 73 us
    ppermute x8, waiting for transfers between devices: 32 us -> 92.8 us  [partner(): lax.ppermute(value, axis, [(i, i ^ 1 << stride) for i in range(lax.axis_s...]
    all_gather x1 -> x0, waiting for transfers between devices: 23.3 us -> none  [per_device(): pieces = lax.all_gather(key_values, 'sp', axis=0, tiled=True)]
    all_to_all x0 -> x1, starting transfers between devices: none -> 6.59 us  [per_device(): lax.all_to_all(jnp.stack([key_values] * lax.axis_size('sp')), 'sp', 0, 0)]
    all_to_all x0 -> x1, local copies, waits for them, and re-layouts: none -> 6.39 us  [per_device(): lax.all_to_all(jnp.stack([key_values] * lax.axis_size('sp')), 'sp', 0, 0)]
    ppermute x8, starting transfers between devices: 9.74 us -> 4.91 us  [partner(): lax.ppermute(value, axis, [(i, i ^ 1 << stride) for i in range(lax.axis_s...]
  transfers between devices with their start and end apart: 10 -> 10, of which waited for: 9 -> 8; matrix products, arithmetic and copies ran while one was open for 0% -> 2% of each run, Pallas kernels for 0% -> 0%
where the time goes in v1:
time: 304 us; the launch traced here: 302 us
  waiting for transfers between devices  98.2 us (32%)
  local copies, waits for them, and re-layouts  73 us (24%)
  matrix products  43.4 us (14%)
  blocking collectives  28 us (9%)
  loops' own time  25.9 us (9%)
  starting transfers between devices  19.7 us (6%)
  other arithmetic  13.5 us (4%)
    ppermute x8, waiting for transfers between devices, partner(): lax.ppermute(value, axis, [(i, i ^ 1 << stride) for i in range(lax.axis_s...  92.8 us
    slice x32, local copies, waits for them, and re-layouts, one_block(): value_slice = pair_slice[:, head_size:]  35.2 us
    another operation x1, loops' own time, per_device(): lax.scan(one_block, state, jnp.arange(piece_rows // key_block, dtype=jnp....  23.4 us
    dynamic_slice x32, local copies, waits for them, and re-layouts, per_device(): lax.scan(one_block, state, jnp.arange(piece_rows // key_block, dtype=jnp....  19.8 us
    dot_general x33, matrix products, attend_step(): jnp.einsum('htu,ud->thd', weights_exp.astype(jnp.bfloat16), value_slice,...  17 us
    dot_general x33, matrix products, attend_step(): jnp.einsum('thd,ud->htu', query_rows, key_slice, preferred_element_type=j...  16.6 us
    all_to_all x1, blocking collectives, per_device(): lax.all_to_all(packed, TP, split_axis=1, concat_axis=0, tiled=True)[:, 0]  14.5 us
    all_to_all x2, blocking collectives, moved_by_axis(): filled = lax.all_to_all(filled, axes[k], k, k, tiled=True)  13.6 us
  transfers between devices with their start and end apart: 10, of which 8 were waited for; matrix products, arithmetic and copies ran while one was open for 2% of the time, Pallas kernels for 0%

profile of v1, /device:TPU:24, one launch (start us, length us, event | category | flops | bytes accessed | tf_op | source)
XLA Modules:
  0.0 302.0 jit_solution(18164895993497804181)
XLA Ops:
  1.3 1.5 multiply_reduce_fusion
  2.8 1.6 convolution_convert_fusion.1
  4.5 3.0 fusion.64
  8.6 14.5 %all_to_all.35 = bf16[128,8,256]{0,2,1:T(8,128)(2,1)S(1)} all-to-all(bf16[128,8,256]{0,2,1:T(8,128)(2,1)S(1)} %pad_maximum_fusion), channel_id=1, replica_groups=mesh['sp'=16,'tp_0'=4,'tp_1'=2] {'tp_0','tp_1'}, dimensions={1} | all-to-all | bytes 1048576 | tf_op jit(solution)/shard_map/all_to_all | solution.py:124
  23.7 8.2 %all-to-all-start.2 = ((f32[16,1024,2]{1,2,0:T(2,128)}), f32[16,1024,2]{1,2,0:T(2,128)S(1)}, u32[]{:S(2)}, u32[]{:S(2)}) async-start(f32[16,1024,2]{1,2,0:T(2,128)} %broadcast_in_dim.53), calls=%async_computation.2 | async-start | bytes 262144 | tf_op jit(solution)/shard_map/all_to_all | solution.py:22
  32.3 5.4 %all-to-all-done.2 = f32[16,1024,2]{1,2,0:T(2,128)S(1)} async-done(((f32[16,1024,2]{1,2,0:T(2,128)}), f32[16,1024,2]{1,2,0:T(2,128)S(1)}, u32[]{:S(2)}, u32[]{:S(2)}) %all-to-all-start.2) | async-done | bytes 131104 | tf_op jit(solution)/shard_map/all_to_all | solution.py:22
  37.7 2.5 stack.2
  40.1 6.6 %all-to-all-start.1 = ((bf16[16,1024,128]{1,2,0:T(8,128)(2,1)}), bf16[16,1024,128]{1,2,0:T(8,128)(2,1)}, u32[]{:S(2)}, u32[]{:S(2)}) async-start(bf16[16,1024,128]{1,2,0:T(8,128)(2,1)} %stack.2), calls=%async_computation.1 | async-start | bytes 8388608 | tf_op jit(solution)/shard_map/all_to_all | solution.py:157
  47.8 59.3 %collective-permute-done = bf16[512,2,64]{0,2,1:T(8,128)(2,1)S(1)} collective-permute-done((bf16[512,2,64]{0,2,1:T(8,128)(2,1)S(1)}, bf16[512,2,64]{0,2,1:T(8,128)(2,1)S(1)}, u32[]{:S(2)}, u32[]{:S(2)}) %collective-permute-start) | collective-permute-done | bytes 131104 | tf_op jit(solution)/shard_map/ppermute | solution.py:32
  107.1 6.5 %collective-permute-done.1 = bf16[512,2,64]{0,2,1:T(8,128)(2,1)S(1)} collective-permute-done((bf16[512,2,64]{0,2,1:T(8,128)(2,1)S(1)}, bf16[512,2,64]{0,2,1:T(8,128)(2,1)S(1)}, u32[]{:S(2)}, u32[]{:S(2)}) %collective-permute-start.1) | collective-permute-done | bytes 131104 | tf_op jit(solution)/shard_map/ppermute | solution.py:32
  113.6 5.0 %collective-permute-done.2 = bf16[512,2,64]{0,2,1:T(8,128)(2,1)S(1)} collective-permute-done((bf16[512,2,64]{0,2,1:T(8,128)(2,1)S(1)}, bf16[512,2,64]{0,2,1:T(8,128)(2,1)S(1)}, u32[]{:S(2)}, u32[]{:S(2)}) %collective-permute-start.2) | collective-permute-done | bytes 131104 | tf_op jit(solution)/shard_map/ppermute | solution.py:32
  118.5 3.2 %collective-permute-start.3 = (bf16[512,2,64]{0,2,1:T(8,128)(2,1)S(1)}, bf16[512,2,64]{0,2,1:T(8,128)(2,1)S(1)}, u32[]{:S(2)}, u32[]{:S(2)}) collective-permute-start(bf16[512,2,64]{0,2,1:T(8,128)(2,1)S(1)} %collective-permute-done.2), channel_id=1, source_target_pairs={{0,64},{8,72},{16,80},{24,88},{32,96},{40,104},{48,112},{56,120},{... | collective-permute-start | bytes 393224 | tf_op jit(solution)/shard_map/ppermute | solution.py:32
  121.8 6.4 %copy.70 = bf16[16,1024,128]{2,1,0:T(8,128)(2,1)} copy(bf16[16,1024,128]{1,2,0:T(8,128)(2,1)} %all-to-all-done.1) | data formatting | bytes 8388608 | tf_op jit(solution)/shard_map/all_to_all | solution.py:157
  128.3 133.0 %while.26 = (s32[]{:T(128)}, f32[2,512]{1,0:T(2,128)S(1)}, f32[2,512]{1,0:T(2,128)S(1)}, f32[512,2,64]{0,2,1:T(8,128)S(1)}, f32[2,512]{1,0:T(2,128)S(1)}, /*inde...) while((s32[]{:T(128)}, f32[2,512]{1,0:T(2,128)S(1)}, ...), condition=%wide.region_18.19_spmd.clone.clone, body=%wide.region_3.18_spmd.clone.clone.sunk | while | flops 280763904 | bytes 16956256 | solution.py:201
  131.0 1.4 conditional.9
  132.4 1.4 conditional.8
  136.4 1.4 conditional.9
  141.8 1.4 conditional.9
  147.3 1.4 conditional.9
  152.7 1.4 conditional.9
  158.2 1.4 conditional.9
  163.6 1.4 conditional.9
  165.1 2.1 conditional.8
  173.9 1.4 conditional.9
  178.0 1.4 conditional.9
  182.0 1.4 conditional.9
  186.1 1.4 conditional.9
  190.2 1.4 conditional.9
  194.2 1.4 conditional.9
  198.3 1.4 conditional.9
  202.4 1.4 conditional.9
  206.4 1.4 conditional.9
  210.5 1.4 conditional.9
  214.6 1.4 conditional.9
  218.6 1.4 conditional.9
  222.7 1.4 conditional.9
  226.8 1.4 conditional.9
  230.8 1.4 conditional.9
  234.9 1.4 conditional.9
  239.0 1.4 conditional.9
  243.0 2.1 conditional.9
  261.5 5.0 %collective-permute-done.4 = bf16[512,2,64]{0,2,1:T(8,128)(2,1)S(1)} collective-permute-done((bf16[512,2,64]{0,2,1:T(8,128)(2,1)S(1)}, bf16[512,2,64]{0,2,1:T(8,128)(2,1)S(1)}, u32[]{:S(2)}, u32[]{:S(2)}) %collective-permute-start.4) | collective-permute-done | bytes 131104 | tf_op jit(solution)/shard_map/ppermute | solution.py:32
  266.8 6.1 %collective-permute-done.5 = bf16[512,2,64]{0,2,1:T(8,128)(2,1)S(1)} collective-permute-done((bf16[512,2,64]{0,2,1:T(8,128)(2,1)S(1)}, bf16[512,2,64]{0,2,1:T(8,128)(2,1)S(1)}, u32[]{:S(2)}, u32[]{:S(2)}) %collective-permute-start.5) | collective-permute-done | bytes 131104 | tf_op jit(solution)/shard_map/ppermute | solution.py:32
  272.9 5.0 %collective-permute-done.6 = bf16[512,2,64]{0,2,1:T(8,128)(2,1)S(1)} collective-permute-done((bf16[512,2,64]{0,2,1:T(8,128)(2,1)S(1)}, bf16[512,2,64]{0,2,1:T(8,128)(2,1)S(1)}, u32[]{:S(2)}, u32[]{:S(2)}) %collective-permute-start.6) | collective-permute-done | bytes 131104 | tf_op jit(solution)/shard_map/ppermute | solution.py:32
  278.3 6.1 %collective-permute-done.7 = bf16[512,2,64]{0,2,1:T(8,128)(2,1)S(1)} collective-permute-done((bf16[512,2,64]{0,2,1:T(8,128)(2,1)S(1)}, bf16[512,2,64]{0,2,1:T(8,128)(2,1)S(1)}, u32[]{:S(2)}, u32[]{:S(2)}) %collective-permute-start.7) | collective-permute-done | bytes 131104 | tf_op jit(solution)/shard_map/ppermute | solution.py:32
  284.6 3.9 %all_to_all.36 = bf16[4,2,128,128]{2,3,0,1:T(8,128)(2,1)S(1)} all-to-all(bf16[4,2,128,128]{2,3,0,1:T(8,128)(2,1)S(1)} %copy.74), channel_id=1, replica_groups=mesh['sp'=16,'tp_0'=4,'tp_1'=2] {'tp_1'}, dimensions={1} | all-to-all | bytes 524288 | tf_op jit(solution)/shard_map/all_to_all | solution.py:44
  288.6 9.6 %all_to_all.37 = bf16[4,2,128,128]{2,3,1,0:T(8,128)(2,1)S(1)} all-to-all(bf16[4,2,128,128]{2,3,1,0:T(8,128)(2,1)S(1)} %copy.75), channel_id=1, replica_groups=mesh['sp'=16,'tp_0'=4,'tp_1'=2] {'tp_0'}, dimensions={0} | all-to-all | bytes 524288 | tf_op jit(solution)/shard_map/all_to_all | solution.py:44
  298.2 3.7 %convolution_convert_fusion = bf16[128,2048]{1,0:T(8,128)(2,1)} fusion(bf16[128,1024]{0,1:T(8,128)(2,1)S(1)} %bitcast.135, bf16[1024,2048]{1,0:T(8,128)(2,1)} %param.25), kind=kOutput, calls=%fused_computation.69 | convolution fusion | flops 537133056 | bytes 4980736 | tf_op jit(solution)/shard_map/dot_general | solution.py:210
  (552 shorter events, 121.7 us)
Async XLA Ops:
  0.0 1.3 copy-start
  0.0 4.4 %copy-start.1 = (bf16[128,2048]{1,0:T(8,128)(2,1)S(1)}, bf16[128,2048]{1,0:T(8,128)(2,1)}, u32[]{:S(2)}) copy-start(bf16[128,2048]{1,0:T(8,128)(2,1)} %param.17) | copy-start | bytes 1572868
  0.0 4.5 %copy-start.2 = (f32[2048]{0:T(1024)S(1)}, f32[2048]{0:T(1024)}, u32[]{:S(2)}) copy-start(f32[2048]{0:T(1024)} %param.18) | copy-start | bytes 24580
  7.4 0.7 copy-start.5
  7.4 0.7 copy-start.4
  8.3 14.7 %copy-start.3 = (f32[1024,2]{0,1:T(2,128)S(1)}, f32[1024,2]{0,1:T(2,128)}, u32[]{:S(2)}) copy-start(f32[1024,2]{0,1:T(2,128)} %param.24) | copy-start | bytes 24580
  23.7 14.0 %all-to-all-start.2 = ((f32[16,1024,2]{1,2,0:T(2,128)}), f32[16,1024,2]{1,2,0:T(2,128)S(1)}, u32[]{:S(2)}, u32[]{:S(2)}) async-start(f32[16,1024,2]{1,2,0:T(2,128)} %broadcast_in_dim.53), calls=%async_computation.2 | async-start | bytes 262144 | tf_op jit(solution)/shard_map/all_to_all | solution.py:22
  40.1 81.7 %all-to-all-start.1 = ((bf16[16,1024,128]{1,2,0:T(8,128)(2,1)}), bf16[16,1024,128]{1,2,0:T(8,128)(2,1)}, u32[]{:S(2)}, u32[]{:S(2)}) async-start(bf16[16,1024,128]{1,2,0:T(8,128)(2,1)} %stack.2), calls=%async_computation.1 | async-start | bytes 8388608 | tf_op jit(solution)/shard_map/all_to_all | solution.py:157
  46.9 60.2 %collective-permute-start = (bf16[512,2,64]{0,2,1:T(8,128)(2,1)S(1)}, bf16[512,2,64]{0,2,1:T(8,128)(2,1)S(1)}, u32[]{:S(2)}, u32[]{:S(2)}) collective-permute-start(bf16[512,2,64]{0,2,1:T(8,128)(2,1)S(1)} %bitcast.141), channel_id=1, source_target_pairs={{0,8},{8,0},{16,24},{24,16},{32,40},{40,32},{48,56},{56,48},{64,72... | collective-permute-start | bytes 393224 | tf_op jit(solution)/shard_map/ppermute | solution.py:32
  107.1 6.5 %collective-permute-start.1 = (bf16[512,2,64]{0,2,1:T(8,128)(2,1)S(1)}, bf16[512,2,64]{0,2,1:T(8,128)(2,1)S(1)}, u32[]{:S(2)}, u32[]{:S(2)}) collective-permute-start(bf16[512,2,64]{0,2,1:T(8,128)(2,1)S(1)} %collective-permute-done), channel_id=1, source_target_pairs={{0,16},{8,24},{16,0},{24,8},{32,48},{40,56},{48,32},{56,40},{64,80... | collective-permute-start | bytes 393224 | tf_op jit(solution)/shard_map/ppermute | solution.py:32
  113.6 5.0 %collective-permute-start.2 = (bf16[512,2,64]{0,2,1:T(8,128)(2,1)S(1)}, bf16[512,2,64]{0,2,1:T(8,128)(2,1)S(1)}, u32[]{:S(2)}, u32[]{:S(2)}) collective-permute-start(bf16[512,2,64]{0,2,1:T(8,128)(2,1)S(1)} %collective-permute-done.1), channel_id=1, source_target_pairs={{0,32},{8,40},{16,48},{24,56},{32,0},{40,8},{48,16},{56,24},{64,96... | collective-permute-start | bytes 393224 | tf_op jit(solution)/shard_map/ppermute | solution.py:32
  118.5 9.7 %collective-permute-start.3 = (bf16[512,2,64]{0,2,1:T(8,128)(2,1)S(1)}, bf16[512,2,64]{0,2,1:T(8,128)(2,1)S(1)}, u32[]{:S(2)}, u32[]{:S(2)}) collective-permute-start(bf16[512,2,64]{0,2,1:T(8,128)(2,1)S(1)} %collective-permute-done.2), channel_id=1, source_target_pairs={{0,64},{8,72},{16,80},{24,88},{32,96},{40,104},{48,112},{56,120},{... | collective-permute-start | bytes 393224 | tf_op jit(solution)/shard_map/ppermute | solution.py:32
  261.4 5.0 %collective-permute-start.4 = (bf16[512,2,64]{0,2,1:T(8,128)(2,1)S(1)}, bf16[512,2,64]{0,2,1:T(8,128)(2,1)S(1)}, u32[]{:S(2)}, u32[]{:S(2)}) collective-permute-start(bf16[512,2,64]{0,2,1:T(8,128)(2,1)S(1)} %divide_convert_fusion), channel_id=1, source_target_pairs={{0,8},{8,0},{16,24},{24,16},{32,40},{40,32},{48,56},{56,48},{64,72... | collective-permute-start | bytes 393224 | tf_op jit(solution)/shard_map/ppermute | solution.py:32
  266.5 6.5 %collective-permute-start.5 = (bf16[512,2,64]{0,2,1:T(8,128)(2,1)S(1)}, bf16[512,2,64]{0,2,1:T(8,128)(2,1)S(1)}, u32[]{:S(2)}, u32[]{:S(2)}) collective-permute-start(bf16[512,2,64]{0,2,1:T(8,128)(2,1)S(1)} %collective-permute-done.4), channel_id=1, source_target_pairs={{0,16},{8,24},{16,0},{24,8},{32,48},{40,56},{48,32},{56,40},{64,80... | collective-permute-start | bytes 393224 | tf_op jit(solution)/shard_map/ppermute | solution.py:32
  272.9 5.0 %collective-permute-start.6 = (bf16[512,2,64]{0,2,1:T(8,128)(2,1)S(1)}, bf16[512,2,64]{0,2,1:T(8,128)(2,1)S(1)}, u32[]{:S(2)}, u32[]{:S(2)}) collective-permute-start(bf16[512,2,64]{0,2,1:T(8,128)(2,1)S(1)} %collective-permute-done.5), channel_id=1, source_target_pairs={{0,32},{8,40},{16,48},{24,56},{32,0},{40,8},{48,16},{56,24},{64,96... | collective-permute-start | bytes 393224 | tf_op jit(solution)/shard_map/ppermute | solution.py:32
  277.9 6.5 %collective-permute-start.7 = (bf16[512,2,64]{0,2,1:T(8,128)(2,1)S(1)}, bf16[512,2,64]{0,2,1:T(8,128)(2,1)S(1)}, u32[]{:S(2)}, u32[]{:S(2)}) collective-permute-start(bf16[512,2,64]{0,2,1:T(8,128)(2,1)S(1)} %collective-permute-done.6), channel_id=1, source_target_pairs={{0,64},{8,72},{16,80},{24,88},{32,96},{40,104},{48,112},{56,120},{... | collective-permute-start | bytes 393224 | tf_op jit(solution)/shard_map/ppermute | solution.py:32
